TPU v7x, 32 devices: a whole 2x2x4 slice. The times are simulated.
32 devices in a mesh: tp: 16 (over z, y, x), dp: 2 (over core).
Axes of the slice: x: 2, y: 2, z: 4, core: 2. Of those that a mesh axis runs over, the one named last changes fastest.
Arguments:
- hidden: bfloat16 [16, 4096], P(None, 'dp'), may hold values from -6 to 6
- norm_gain: float32 [2, 4096], P(None, 'dp'), may hold values from 0.1 to 1.9
- gate_weight: bfloat16 [2, 4096, 8192], P(None, 'dp', 'tp'), may hold values from -0.09375 to 0.09375
- inner_weight: bfloat16 [2, 4096, 8192], P(None, 'dp', 'tp'), may hold values from -0.09375 to 0.09375
- write_weight: bfloat16 [2, 4096, 2048], P(None, 'dp', 'tp'), may hold values from -0.09375 to 0.09375
- read_weight: bfloat16 [2, 4096, 2048], P(None, 'dp', 'tp'), may hold values from -0.09375 to 0.09375
- step_weight: bfloat16 [2, 4096, 128], P(None, 'dp'), may hold values from -0.09375 to 0.09375
- conv_inner: bfloat16 [2, 4, 8192], P(None, None, 'tp'), may hold values from -3 to 3
- conv_write: bfloat16 [2, 4, 2048], P(None, None, 'tp'), may hold values from -3 to 3
- conv_read: bfloat16 [2, 4, 2048], P(None, None, 'tp'), may hold values from -3 to 3
- step_bias: float32 [2, 128], P(None, 'tp'), may hold values from -4 to -1
- decay_log: float32 [2, 128], P(None, 'tp'), may hold values from -3 to 0.5
- skip_gain: float32 [2, 128], P(None, 'tp'), may hold values from 0.1 to 1.9
- group_gain: float32 [2, 8192], P(None, 'tp'), may hold values from 0.1 to 1.9
- out_weight: bfloat16 [2, 8192, 4096], P(None, 'tp', 'dp'), may hold values from -0.4 to 0.4
- state_inner: bfloat16 [2, 16, 3, 8192], P(None, 'dp', None, 'tp'), may hold values from -6 to 6
- state_write: bfloat16 [2, 16, 3, 2048], P(None, 'dp', None, 'tp'), may hold values from -6 to 6
- state_read: bfloat16 [2, 16, 3, 2048], P(None, 'dp', None, 'tp'), may hold values from -6 to 6
- recurrent: float32 [2, 16, 128, 64, 128], P(None, 'dp', 'tp'), may hold values from -1.2 to 1.2, as said below
Outputs:
- out_hidden: bfloat16 [16, 4096], P(None, 'dp')
- next_inner: bfloat16 [2, 16, 3, 8192], P(None, 'dp', None, 'tp')
- next_write: bfloat16 [2, 16, 3, 2048], P(None, 'dp', None, 'tp')
- next_read: bfloat16 [2, 16, 3, 2048], P(None, 'dp', None, 'tp')
- next_recurrent: float32 [2, 16, 128, 64, 128], P(None, 'dp', 'tp')
Inputs may be any that keep to these rules, and one draw needn't show every extreme that they name: recurrent states of order a tenth, with scales that differ between heads.
All inputs are finite; a program needn't handle non-finite values.
Results may differ from a plain program's by a relative error of at most 0.025.
Values may be sent and summed in bfloat16 or wider, within the bound.
A program may use at most 64 MiB of HBM per device.

v0:
```python
import jax
import jax.numpy as jnp
from jax import lax
from jax.sharding import PartitionSpec as P

D = 4096
HEADS = 128
GROUPS = 16
eps = 1e-06


def convolve(state, fresh_row, kernel):
    window = jnp.concatenate([state, fresh_row[:, None, :]], axis=1)
    summed = jnp.sum(window.astype(jnp.float32) * kernel.astype(jnp.float32)[None], axis=1)
    return (jax.nn.silu(summed), window[:, 1:])


def mixer_block(normed, number, weights):
    (
        gate_weight,
        inner_weight,
        write_weight,
        read_weight,
        step_weight,
        conv_inner,
        conv_write,
        conv_read,
        step_bias,
        decay_log,
        skip_gain,
        group_gain,
        out_weight,
        state_inner,
        state_write,
        state_read,
        recurrent,
    ) = weights

    def partial_of(weight):
        return jnp.dot(normed, weight[number], preferred_element_type=jnp.float32).astype(
            jnp.bfloat16
        )

    summed = (
        lax.psum_scatter(partial_of(gate_weight), "dp", scatter_dimension=0, tiled=True).astype(
            jnp.float32
        ),
        lax.psum_scatter(partial_of(inner_weight), "dp", scatter_dimension=0, tiled=True).astype(
            jnp.float32
        ),
        lax.psum_scatter(partial_of(write_weight), "dp", scatter_dimension=0, tiled=True).astype(
            jnp.float32
        ),
        lax.psum_scatter(partial_of(read_weight), "dp", scatter_dimension=0, tiled=True).astype(
            jnp.float32
        ),
        lax.psum_scatter(partial_of(step_weight), "dp", scatter_dimension=0, tiled=True).astype(
            jnp.float32
        ),
    )
    gate_raw, inner_raw, write_raw, read_raw, step_raw = [
        member.astype(jnp.bfloat16) for member in summed
    ]
    inner_act, next_inner = convolve(state_inner[number], inner_raw, conv_inner[number])
    write_act, next_write = convolve(state_write[number], write_raw, conv_write[number])
    read_act, next_read = convolve(state_read[number], read_raw, conv_read[number])
    write_all, read_all = (
        lax.all_gather(write_act.astype(jnp.bfloat16), "tp", axis=1, tiled=True),
        lax.all_gather(read_act.astype(jnp.bfloat16), "tp", axis=1, tiled=True),
    )
    heads_here = step_bias.shape[1]
    head_dim = recurrent.shape[3]
    state_dim = recurrent.shape[4]
    rows_here = inner_act.shape[0]
    first_head = lax.axis_index("tp") * heads_here
    group_index = first_head // (HEADS // GROUPS)
    write_grid = write_all.reshape(rows_here, state_dim, GROUPS)
    read_grid = read_all.reshape(rows_here, state_dim, GROUPS)
    write_vec = lax.dynamic_slice_in_dim(write_grid, group_index, 1, 2)[:, :, 0].astype(jnp.float32)
    read_vec = lax.dynamic_slice_in_dim(read_grid, group_index, 1, 2)[:, :, 0].astype(jnp.float32)
    step_own = lax.dynamic_slice_in_dim(step_raw, first_head, heads_here, 1)
    step_size = jax.nn.softplus(step_own.astype(jnp.float32) + step_bias[number][None, :])
    retain = jnp.exp(-step_size * jnp.exp(decay_log[number])[None, :])
    inner_heads = inner_act.reshape(rows_here, heads_here, head_dim)
    updated = (
        retain[:, :, None, None] * recurrent[number]
        + (step_size[:, :, None] * inner_heads)[:, :, :, None] * write_vec[:, None, None, :]
    )
    readout = jnp.einsum("bhpn,bn->bhp", updated, read_vec, precision=lax.Precision.HIGHEST)
    readout = readout + skip_gain[number][None, :, None] * inner_heads
    gated_out = readout.reshape(rows_here, heads_here * head_dim) * jax.nn.silu(
        gate_raw.astype(jnp.float32)
    )
    selector = (jnp.arange(GROUPS) == group_index).astype(jnp.float32)
    totals = lax.psum(jnp.sum(gated_out * gated_out, axis=1)[:, None] * selector[None, :], "tp")
    group_sum = jnp.sum(totals * selector[None, :], axis=1, keepdims=True)
    group_factor = lax.rsqrt(group_sum / (HEADS // GROUPS * head_dim) + eps)
    group_normed = (gated_out * group_factor * group_gain[number][None, :]).astype(jnp.bfloat16)
    branch = jnp.dot(
        lax.all_gather(group_normed, "dp", axis=0, tiled=True),
        out_weight[number],
        preferred_element_type=jnp.float32,
    )
    return (branch, (next_inner, next_write, next_read, updated))


def total_over(branch):
    return lax.psum(branch, "tp")


def local(
    hidden,
    norm_gain,
    gate_weight,
    inner_weight,
    write_weight,
    read_weight,
    step_weight,
    conv_inner,
    conv_write,
    conv_read,
    step_bias,
    decay_log,
    skip_gain,
    group_gain,
    out_weight,
    state_inner,
    state_write,
    state_read,
    recurrent,
):
    weights = (
        gate_weight,
        inner_weight,
        write_weight,
        read_weight,
        step_weight,
        conv_inner,
        conv_write,
        conv_read,
        step_bias,
        decay_log,
        skip_gain,
        group_gain,
        out_weight,
        state_inner,
        state_write,
        state_read,
        recurrent,
    )
    wide_in = hidden.astype(jnp.float32)
    squares = lax.psum(jnp.sum(wide_in * wide_in, axis=1, keepdims=True), "dp")
    normed = (wide_in * lax.rsqrt(squares / D + eps) * norm_gain[0][None, :]).astype(jnp.bfloat16)
    branch, first_states = mixer_block(normed, 0, weights)
    middle = (wide_in + total_over(branch)).astype(jnp.bfloat16).astype(jnp.float32)
    squares = lax.psum(jnp.sum(middle * middle, axis=1, keepdims=True), "dp")
    normed = (middle * lax.rsqrt(squares / D + eps) * norm_gain[1][None, :]).astype(jnp.bfloat16)
    branch, second_states = mixer_block(normed, 1, weights)
    result = (middle + total_over(branch)).astype(jnp.bfloat16)
    stacked = [jnp.stack([earlier, later]) for earlier, later in zip(first_states, second_states)]
    return (result, stacked[0], stacked[1], stacked[2], stacked[3])


def solution(mesh):
    return jax.shard_map(
        local,
        mesh=mesh,
        in_specs=(
            P(None, "dp"),
            P(None, "dp"),
            P(None, "dp", "tp"),
            P(None, "dp", "tp"),
            P(None, "dp", "tp"),
            P(None, "dp", "tp"),
            P(None, "dp", None),
            P(None, None, "tp"),
            P(None, None, "tp"),
            P(None, None, "tp"),
            P(None, "tp"),
            P(None, "tp"),
            P(None, "tp"),
            P(None, "tp"),
            P(None, "tp", "dp"),
            P(None, "dp", None, "tp"),
            P(None, "dp", None, "tp"),
            P(None, "dp", None, "tp"),
            P(None, "dp", "tp", None, None),
        ),
        out_specs=(
            P(None, "dp"),
            P(None, "dp", None, "tp"),
            P(None, "dp", None, "tp"),
            P(None, "dp", None, "tp"),
            P(None, "dp", "tp", None, None),
        ),
        check_vma=False,
    )
```

profile of v0, /device:TPU:0, one launch (start us, length us, event | category | flops | bytes accessed | tf_op | source)
XLA Modules:
  0.0 509.0 jit_solution(9227752754220769065)
XLA Ops:
  7.2 1.0 fusion.58
  8.2 2.6 psum.42
  10.8 0.8 fusion.97
  11.8 2.8 fusion.28
  14.7 2.6 fusion.31
  17.4 0.6 dynamic-slice
  18.8 0.2 convolution_convert_fusion.4
  19.1 0.2 convolution_convert_fusion.3
  19.3 1.3 convolution_convert_fusion.5
  20.6 3.5 all-reduce.7
  24.2 42.2 %all_gather.18 = bf16[8,2048]{1,0:T(8,128)(2,1)S(1)} all-gather(bf16[8,128]{1,0:T(8,128)(2,1)S(1)} %multiply_convert_fusion.5), channel_id=1, replica_groups=mesh['tp'=16,'dp'=2] {'tp'}, dimensions={1}, use_global_device_ids=true | all-gather | bytes 34816 | tf_op jit(solution)/shard_map/all_gather | solution.py:68
  66.4 35.6 %all_gather.19 = bf16[8,2048]{1,0:T(8,128)(2,1)S(1)} all-gather(bf16[8,128]{1,0:T(8,128)(2,1)S(1)} %multiply_convert_fusion.4), channel_id=1, replica_groups=mesh['tp'=16,'dp'=2] {'tp'}, dimensions={1}, use_global_device_ids=true | all-gather | bytes 34816 | tf_op jit(solution)/shard_map/all_gather | solution.py:69
  102.2 0.3 dynamic-slice_reduce_fusion.1
  102.7 0.2 convert_reduce_fusion.1
  103.2 0.7 multiply_reduce_fusion.1
  104.0 4.2 fusion.16
  108.4 0.8 multiply_reduce_fusion.5
  109.3 38.6 %psum.43 = f32[8,16]{1,0:T(8,128)S(1)} all-reduce(f32[8,16]{1,0:T(8,128)S(1)} %broadcast_multiply_fusion.3), channel_id=1, replica_groups=mesh['tp'=16,'dp'=2] {'tp'}, use_global_device_ids=true, to_apply=%region_11.12 | all-reduce | flops 128 | bytes 1024 | tf_op jit(solution)/shard_map/psum | solution.py:95
  148.0 0.8 multiply_convert_fusion.1
  148.8 1.8 all_gather.20
  150.6 2.6 fusion.9
  153.4 101.5 %all-reduce.11.cloned.1.call-done = f32[16,2048]{1,0:T(8,128)} async-done(((f32[16,2048]{1,0:T(8,128)}), f32[16,2048]{1,0:T(8,128)}) %all-reduce.11.cloned.1.call-update) | async-done | bytes 131088 | tf_op jit(solution)/shard_map/psum | solution.py:108
  254.8 1.0 fusion.62
  255.9 2.5 psum.45
  258.4 0.2 convolution_convert_fusion.1
  258.6 0.2 convolution_convert_fusion
  258.8 1.3 convolution_convert_fusion.2
  260.1 2.6 fusion.34
  262.8 2.6 fusion.37
  265.4 3.3 all-reduce.6
  268.8 0.6 pad_maximum_fusion.4
  269.5 0.6 pad_maximum_fusion.5
  270.1 38.9 %all_gather.21 = bf16[8,2048]{1,0:T(8,128)(2,1)S(1)} all-gather(bf16[8,128]{1,0:T(8,128)(2,1)S(1)} %multiply_convert_fusion.3), channel_id=1, replica_groups=mesh['tp'=16,'dp'=2] {'tp'}, dimensions={1}, use_global_device_ids=true | all-gather | bytes 34816 | tf_op jit(solution)/shard_map/all_gather | solution.py:68
  309.1 35.6 %all_gather.22 = bf16[8,2048]{1,0:T(8,128)(2,1)S(1)} all-gather(bf16[8,128]{1,0:T(8,128)(2,1)S(1)} %multiply_convert_fusion.2), channel_id=1, replica_groups=mesh['tp'=16,'dp'=2] {'tp'}, dimensions={1}, use_global_device_ids=true | all-gather | bytes 34816 | tf_op jit(solution)/shard_map/all_gather | solution.py:69
  345.0 0.3 dynamic-slice_reduce_fusion
  345.3 0.3 convert_reduce_fusion
  345.7 0.7 multiply_reduce_fusion
  346.6 4.2 multiply_add_fusion.1
  350.8 2.8 fusion.7
  353.8 0.8 multiply_reduce_fusion.2
  354.7 39.1 %psum.46 = f32[8,16]{1,0:T(8,128)S(1)} all-reduce(f32[8,16]{1,0:T(8,128)S(1)} %broadcast_multiply_fusion.2), channel_id=1, replica_groups=mesh['tp'=16,'dp'=2] {'tp'}, use_global_device_ids=true, to_apply=%region_25.26 | all-reduce | flops 128 | bytes 1024 | tf_op jit(solution)/shard_map/psum | solution.py:95
  393.9 0.8 multiply_convert_fusion
  394.7 1.8 all_gather.23
  396.5 2.6 fusion
  399.1 4.1 pad_maximum_fusion
  403.2 0.6 pad_maximum_fusion.1
  403.8 96.8 %all-reduce.13.cloned.1.call-done = f32[16,2048]{1,0:T(8,128)} async-done(((f32[16,2048]{1,0:T(8,128)}), f32[16,2048]{1,0:T(8,128)}) %all-reduce.13.cloned.1.call-update) | async-done | bytes 131088 | tf_op jit(solution)/shard_map/psum | solution.py:108
  500.6 1.6 fusion.65
  (101 shorter events, 2.8 us)
Async XLA Ops:
  7.2 7.5 %copy-start.1 = (bf16[16,2048]{1,0:T(8,128)(2,1)S(1)}, bf16[16,2048]{1,0:T(8,128)(2,1)}, u32[]{:S(2)}) copy-start(bf16[16,2048]{1,0:T(8,128)(2,1)} %param.19) | copy-start | bytes 196612
  7.2 96.0 %reduce-scatter.5.cloned.1.call-start = ((), (), s32[]{:S(2)}) async-start(), calls=%async_computation.4 | async-start | bytes 24576 | tf_op jit(solution)/shard_map/reduce_scatter | solution.py:48
  11.7 5.8 %copy-start.16 = (u32[32]{0:T(128)S(1)}, u32[32]{0:T(128)}, u32[]{:S(2)}) copy-start(u32[32]{0:T(128)} %constant.63) | copy-start | bytes 388
  11.7 7.0 %copy-start.11 = (f32[2,8]{1,0:T(2,128)S(1)}, f32[2,8]{1,0:T(2,128)}, u32[]{:S(2)}) copy-start(f32[2,8]{1,0:T(2,128)} %param.31) | copy-start | bytes 196
  11.7 7.0 %copy-start.9 = (bf16[2,4,128]{2,1,0:T(4,128)(2,1)S(1)}, bf16[2,4,128]{2,1,0:T(4,128)(2,1)}, u32[]{:S(2)}) copy-start(bf16[2,4,128]{2,1,0:T(4,128)(2,1)} %param.27) | copy-start | bytes 6148
  11.7 7.0 %copy-start.10 = (bf16[2,4,128]{2,1,0:T(4,128)(2,1)S(1)}, bf16[2,4,128]{2,1,0:T(4,128)(2,1)}, u32[]{:S(2)}) copy-start(bf16[2,4,128]{2,1,0:T(4,128)(2,1)} %param.28) | copy-start | bytes 6148
  11.7 7.0 %copy-start.8 = (f32[2,512]{1,0:T(2,128)S(1)}, f32[2,512]{1,0:T(2,128)}, u32[]{:S(2)}) copy-start(f32[2,512]{1,0:T(2,128)} %param.32) | copy-start | bytes 12292
  11.7 7.1 %copy-start.5 = (bf16[2,8,3,128]{3,1,2,0:T(8,128)(2,1)S(1)}, bf16[2,8,3,128]{3,1,2,0:T(8,128)(2,1)}, u32[]{:S(2)}) copy-start(bf16[2,8,3,128]{3,1,2,0:T(8,128)(2,1)} %param.35) | copy-start | bytes 36868
  11.7 7.1 %copy-start.6 = (bf16[2,8,3,128]{3,1,2,0:T(8,128)(2,1)S(1)}, bf16[2,8,3,128]{3,1,2,0:T(8,128)(2,1)}, u32[]{:S(2)}) copy-start(bf16[2,8,3,128]{3,1,2,0:T(8,128)(2,1)} %param.36) | copy-start | bytes 36868
  11.7 7.1 %copy-start.14 = (bf16[2,2048,128]{2,1,0:T(8,128)(2,1)S(1)}, bf16[2,2048,128]{2,1,0:T(8,128)(2,1)}, u32[]{:S(2)}) copy-start(bf16[2,2048,128]{2,1,0:T(8,128)(2,1)} %param.23) | copy-start | bytes 3145732
  11.8 7.3 %copy-start.15 = (bf16[2,2048,128]{2,1,0:T(8,128)(2,1)S(1)}, bf16[2,2048,128]{2,1,0:T(8,128)(2,1)}, u32[]{:S(2)}) copy-start(bf16[2,2048,128]{2,1,0:T(8,128)(2,1)} %param.24) | copy-start | bytes 3145732
  14.6 9.5 %copy-start.7 = (bf16[2,4,512]{2,1,0:T(4,128)(2,1)S(1)}, bf16[2,4,512]{2,1,0:T(4,128)(2,1)}, u32[]{:S(2)}) copy-start(bf16[2,4,512]{2,1,0:T(4,128)(2,1)} %param.26) | copy-start | bytes 24580
  14.6 87.4 %copy-start.2 = (bf16[2,8,3,512]{3,1,2,0:T(8,128)(2,1)S(1)}, bf16[2,8,3,512]{3,1,2,0:T(8,128)(2,1)}, u32[]{:S(2)}) copy-start(bf16[2,8,3,512]{3,1,2,0:T(8,128)(2,1)} %param.34) | copy-start | bytes 147460
  14.6 93.8 %reduce-scatter.7.cloned.1.call-start = ((), (), s32[]{:S(2)}) async-start(), calls=%async_computation.5 | async-start | bytes 24576 | tf_op jit(solution)/shard_map/reduce_scatter | solution.py:45
  17.3 85.7 %copy-start.12 = (f32[2,8]{1,0:T(2,128)S(1)}, f32[2,8]{1,0:T(2,128)}, u32[]{:S(2)}) copy-start(f32[2,8]{1,0:T(2,128)} %param.30) | copy-start | bytes 196
  17.3 85.7 %copy-start.13 = (f32[2,8]{1,0:T(2,128)S(1)}, f32[2,8]{1,0:T(2,128)}, u32[]{:S(2)}) copy-start(f32[2,8]{1,0:T(2,128)} %param.29) | copy-start | bytes 196
  17.3 237.5 %all-reduce.11.cloned.1.call-start = ((), (), s32[]{:S(2)}) async-start(), calls=%async_computation.6 | async-start | bytes 262144 | tf_op jit(solution)/shard_map/psum | solution.py:108
  104.0 49.3 %copy-start.3 = (bf16[8,512]{1,0:T(8,128)(2,1)S(1)}, bf16[8,512]{1,0:T(8,128)(2,1)}, u32[]{:S(2)}) copy-start(bf16[8,512]{1,0:T(8,128)(2,1)} %reduce-scatter.5.cloned.1.call-done) | copy-start | bytes 24580
  153.3 192.4 %reduce-scatter.9.cloned.1.call-start = ((), (), s32[]{:S(2)}) async-start(), calls=%async_computation.7 | async-start | bytes 24576 | tf_op jit(solution)/shard_map/reduce_scatter | solution.py:48
  268.8 85.0 %reduce-scatter.11.cloned.1.call-start = ((), (), s32[]{:S(2)}) async-start(), calls=%async_computation.8 | async-start | bytes 24576 | tf_op jit(solution)/shard_map/reduce_scatter | solution.py:45
  345.5 155.1 %all-reduce.13.cloned.1.call-start = ((), (), s32[]{:S(2)}) async-start(), calls=%async_computation.9 | async-start | bytes 262144 | tf_op jit(solution)/shard_map/psum | solution.py:108
  346.6 4.2 copy-start
  399.1 4.1 copy-start.4
Sparse Core Ops, SparseCore 0:
  14.7 10.0 reduce-scatter.4
  27.6 8.6 reduce-scatter.6
  153.4 101.3 all-reduce.10
  268.9 6.5 reduce-scatter.8
  345.7 5.2 reduce-scatter.10
  399.3 101.3 all-reduce.12
where the time goes:
time: 510 us; the launch traced here: 509 us
  blocking collectives  245 us (48%)
  waiting for transfers between devices  198 us (39%)
  matrix products  26.6 us (5%)
  other arithmetic  19.8 us (4%)
  between operations  15.3 us (3%)
    psum x2, waiting for transfers between devices, total_over(): return lax.psum(branch, 'tp')  198 us
    all_gather x2, blocking collectives, mixer_block(): lax.all_gather(write_act.astype(jnp.bfloat16), 'tp', axis=1, tiled=True)  81.1 us
    psum x2, blocking collectives, mixer_block(): lax.psum(jnp.sum(gated_out * gated_out, axis=1)[:, None] * selector[None,...  77.7 us
    all_gather x2, blocking collectives, mixer_block(): lax.all_gather(read_act.astype(jnp.bfloat16), 'tp', axis=1, tiled=True)  71.2 us
    dot_general x10, matrix products, partial_of(): jnp.dot(normed, weight[number], preferred_element_type=jnp.float32)  14.2 us
  transfers between devices with their start and end apart: 6, of which 2 were waited for; matrix products, arithmetic and copies ran while one was open for 5% of the time, Pallas kernels for 0%

commit v1 on v0

--- a/solution.py
+++ b/solution.py
@@ -105,7 +105,7 @@
 
 
 def total_over(branch):
-    return lax.psum(branch, "tp")
+    return jnp.sum(lax.all_gather(branch, "tp"), axis=0)
 
 
 def local(

time: 510 us -> 420 us (0.82)
  waiting for transfers between devices: 198 us -> 105 us
    psum x2 -> x0, waiting for transfers between devices: 198 us -> none  [total_over(): return lax.psum(branch, 'tp')]
    all_gather x0 -> x2, waiting for transfers between devices: none -> 105 us  [total_over(): return jnp.sum(lax.all_gather(branch, 'tp'), axis=0)]
  transfers between devices with their start and end apart: 6 -> 6, of which waited for: 2 -> 2; matrix products, arithmetic and copies ran while one was open for 5% -> 6% of each run, Pallas kernels for 0% -> 0%
where the time goes in v1:
time: 420 us; the launch traced here: 419 us
  blocking collectives  248 us (59%)
  waiting for transfers between devices  105 us (25%)
  matrix products  28 us (7%)
  other arithmetic  19.2 us (5%)
  between operations  15.3 us (4%)
    all_gather x2, waiting for transfers between devices, total_over(): return jnp.sum(lax.all_gather(branch, 'tp'), axis=0)  105 us
    all_gather x2, blocking collectives, mixer_block(): lax.all_gather(write_act.astype(jnp.bfloat16), 'tp', axis=1, tiled=True)  80.9 us
    psum x2, blocking collectives, mixer_block(): lax.psum(jnp.sum(gated_out * gated_out, axis=1)[:, None] * selector[None,...  80.4 us
    all_gather x2, blocking collectives, mixer_block(): lax.all_gather(read_act.astype(jnp.bfloat16), 'tp', axis=1, tiled=True)  71.2 us
    dot_general x10, matrix products, partial_of(): jnp.dot(normed, weight[number], preferred_element_type=jnp.float32)  14.2 us
    dot_general x2, matrix products, mixer_block(): jnp.einsum('bhpn,bn->bhp', updated, read_vec, precision=lax.Precision.HIG...  8.47 us
  transfers between devices with their start and end apart: 6, of which 2 were waited for; matrix products, arithmetic and copies ran while one was open for 6% of the time, Pallas kernels for 0%

profile of v1, /device:TPU:0, one launch (start us, length us, event | category | flops | bytes accessed | tf_op | source)
XLA Modules:
  0.0 419.0 jit_solution(10809501237007804426)
XLA Ops:
  7.2 1.0 fusion.58
  8.2 2.6 psum.28
  10.8 0.8 fusion.97
  11.8 2.8 fusion.28
  14.7 2.6 fusion.31
  17.4 0.6 dynamic-slice
  19.1 0.2 convolution_convert_fusion.3
  19.3 1.3 convolution_convert_fusion.5
  20.6 3.5 all-reduce.7
  24.1 42.2 %all_gather.30 = bf16[8,2048]{1,0:T(8,128)(2,1)S(1)} all-gather(bf16[8,128]{1,0:T(8,128)(2,1)S(1)} %multiply_convert_fusion.5), channel_id=1, replica_groups=mesh['tp'=16,'dp'=2] {'tp'}, dimensions={1}, use_global_device_ids=true | all-gather | bytes 34816 | tf_op jit(solution)/shard_map/all_gather | solution.py:68
  66.4 35.6 %all_gather.31 = bf16[8,2048]{1,0:T(8,128)(2,1)S(1)} all-gather(bf16[8,128]{1,0:T(8,128)(2,1)S(1)} %multiply_convert_fusion.4), channel_id=1, replica_groups=mesh['tp'=16,'dp'=2] {'tp'}, dimensions={1}, use_global_device_ids=true | all-gather | bytes 34816 | tf_op jit(solution)/shard_map/all_gather | solution.py:69
  102.2 0.3 dynamic-slice_reduce_fusion.1
  102.7 0.2 convert_reduce_fusion.1
  103.1 0.7 multiply_reduce_fusion.1
  104.0 4.2 %fusion.16 = f32[8,1,8,64]{3,1,2,0:T(1,128)S(1)} fusion(bf16[8,128,1,1]{1,2,3,0:T(2,128)(2,1)S(1)} %reshape.128, f32[2,8,8,64,128]{4,3,2,1,0:T(8,128)} %param.37, f32[8,128]{1,0:T(8,128)S(1)} %convert_reduce_fusion.1, f32[8,8,64]{2,1,0:T(8,128)S(1)} %broadcast_multiply_fusion.1, f32[8,8]{1,0:T(8,128)S(1)} %get-tuple-element.27), kind=kOutput, calls=%fused_computation.18 | convolution fusion | flops 7864320 | bytes 2136320 | tf_op jit(solution)/shard_map/bhpn,bn->bhp/dot_general | solution.py:89
  108.4 0.8 multiply_reduce_fusion.5
  109.3 38.6 %psum.29 = f32[8,16]{1,0:T(8,128)S(1)} all-reduce(f32[8,16]{1,0:T(8,128)S(1)} %broadcast_multiply_fusion.3), channel_id=1, replica_groups=mesh['tp'=16,'dp'=2] {'tp'}, use_global_device_ids=true, to_apply=%region_11.12 | all-reduce | flops 128 | bytes 1024 | tf_op jit(solution)/shard_map/psum | solution.py:95
  148.0 0.8 multiply_convert_fusion.1
  148.8 1.8 all_gather.32
  150.6 2.6 fusion.9
  153.3 56.4 %all-gather.5.cloned.1.call-done = f32[256,2048]{1,0:T(8,128)} async-done(((f32[16,2048]{1,0:T(8,128)}), f32[256,2048]{1,0:T(8,128)}) %all-gather.5.cloned.1.call-update) | async-done | bytes 2097168 | tf_op jit(solution)/shard_map/all_gather | solution.py:108
  209.7 1.7 reduce_sum.137
  211.5 2.5 psum.30
  214.0 0.2 convolution_convert_fusion.1
  214.3 0.2 convolution_convert_fusion
  214.5 1.3 convolution_convert_fusion.2
  215.8 2.6 fusion.34
  218.4 2.6 fusion.37
  221.0 3.3 all-reduce.6
  224.5 38.6 %all_gather.35 = bf16[8,2048]{1,0:T(8,128)(2,1)S(1)} all-gather(bf16[8,128]{1,0:T(8,128)(2,1)S(1)} %multiply_convert_fusion.3), channel_id=1, replica_groups=mesh['tp'=16,'dp'=2] {'tp'}, dimensions={1}, use_global_device_ids=true | all-gather | bytes 34816 | tf_op jit(solution)/shard_map/all_gather | solution.py:68
  263.3 35.6 %all_gather.36 = bf16[8,2048]{1,0:T(8,128)(2,1)S(1)} all-gather(bf16[8,128]{1,0:T(8,128)(2,1)S(1)} %multiply_convert_fusion.2), channel_id=1, replica_groups=mesh['tp'=16,'dp'=2] {'tp'}, dimensions={1}, use_global_device_ids=true | all-gather | bytes 34816 | tf_op jit(solution)/shard_map/all_gather | solution.py:69
  299.2 0.3 dynamic-slice_reduce_fusion
  299.5 0.3 convert_reduce_fusion
  299.9 0.7 multiply_reduce_fusion
  300.8 4.2 %fusion.7 = f32[8,1,8,64]{3,1,2,0:T(1,128)S(1)} fusion(bf16[8,128,1,1]{1,2,3,0:T(2,128)(2,1)S(1)} %reshape.130, f32[2,8,8,64,128]{4,3,2,1,0:T(8,128)} %param.37, f32[8,128]{1,0:T(8,128)S(1)} %convert_reduce_fusion, f32[8,8,64]{2,1,0:T(8,128)S(1)} %broadcast_multiply_fusion, f32[8,8]{1,0:T(8,128)S(1)} %get-tuple-element.25), kind=kOutput, calls=%fused_computation.9 | convolution fusion | flops 7864320 | bytes 2136320 | tf_op jit(solution)/shard_map/bhpn,bn->bhp/dot_general | solution.py:89
  305.2 0.8 multiply_reduce_fusion.2
  306.1 41.9 %psum.31 = f32[8,16]{1,0:T(8,128)S(1)} all-reduce(f32[8,16]{1,0:T(8,128)S(1)} %broadcast_multiply_fusion.2), channel_id=1, replica_groups=mesh['tp'=16,'dp'=2] {'tp'}, use_global_device_ids=true, to_apply=%region_25.26 | all-reduce | flops 128 | bytes 1024 | tf_op jit(solution)/shard_map/psum | solution.py:95
  348.1 0.8 multiply_convert_fusion
  348.9 1.8 all_gather.37
  350.7 2.6 fusion
  353.4 0.6 pad_maximum_fusion.4
  354.0 0.6 pad_maximum_fusion.5
  354.6 0.6 pad_maximum_fusion.1
  355.2 3.7 multiply_add_fusion.1
  358.9 2.3 pad_maximum_fusion
  361.2 48.5 %all-gather.7.cloned.1.call-done = f32[256,2048]{1,0:T(8,128)} async-done(((f32[16,2048]{1,0:T(8,128)}), f32[256,2048]{1,0:T(8,128)}) %all-gather.7.cloned.1.call-update) | async-done | bytes 2097168 | tf_op jit(solution)/shard_map/all_gather | solution.py:108
  409.8 1.7 reduce_sum.145
  411.5 0.7 fusion.65
  (101 shorter events, 3.1 us)
Async XLA Ops:
  7.2 7.5 %copy-start = (bf16[16,2048]{1,0:T(8,128)(2,1)S(1)}, bf16[16,2048]{1,0:T(8,128)(2,1)}, u32[]{:S(2)}) copy-start(bf16[16,2048]{1,0:T(8,128)(2,1)} %param.19) | copy-start | bytes 196612
  7.2 96.0 %reduce-scatter.5.cloned.1.call-start = ((), (), s32[]{:S(2)}) async-start(), calls=%async_computation.4 | async-start | bytes 24576 | tf_op jit(solution)/shard_map/reduce_scatter | solution.py:48
  11.7 5.8 %copy-start.15 = (u32[32]{0:T(128)S(1)}, u32[32]{0:T(128)}, u32[]{:S(2)}) copy-start(u32[32]{0:T(128)} %constant.63) | copy-start | bytes 388
  11.7 7.0 %copy-start.10 = (f32[2,8]{1,0:T(2,128)S(1)}, f32[2,8]{1,0:T(2,128)}, u32[]{:S(2)}) copy-start(f32[2,8]{1,0:T(2,128)} %param.31) | copy-start | bytes 196
  11.7 7.0 %copy-start.8 = (bf16[2,4,128]{2,1,0:T(4,128)(2,1)S(1)}, bf16[2,4,128]{2,1,0:T(4,128)(2,1)}, u32[]{:S(2)}) copy-start(bf16[2,4,128]{2,1,0:T(4,128)(2,1)} %param.27) | copy-start | bytes 6148
  11.7 7.0 %copy-start.9 = (bf16[2,4,128]{2,1,0:T(4,128)(2,1)S(1)}, bf16[2,4,128]{2,1,0:T(4,128)(2,1)}, u32[]{:S(2)}) copy-start(bf16[2,4,128]{2,1,0:T(4,128)(2,1)} %param.28) | copy-start | bytes 6148
  11.7 7.0 %copy-start.7 = (f32[2,512]{1,0:T(2,128)S(1)}, f32[2,512]{1,0:T(2,128)}, u32[]{:S(2)}) copy-start(f32[2,512]{1,0:T(2,128)} %param.32) | copy-start | bytes 12292
  11.7 7.1 %copy-start.4 = (bf16[2,8,3,128]{3,1,2,0:T(8,128)(2,1)S(1)}, bf16[2,8,3,128]{3,1,2,0:T(8,128)(2,1)}, u32[]{:S(2)}) copy-start(bf16[2,8,3,128]{3,1,2,0:T(8,128)(2,1)} %param.35) | copy-start | bytes 36868
  11.7 7.1 %copy-start.5 = (bf16[2,8,3,128]{3,1,2,0:T(8,128)(2,1)S(1)}, bf16[2,8,3,128]{3,1,2,0:T(8,128)(2,1)}, u32[]{:S(2)}) copy-start(bf16[2,8,3,128]{3,1,2,0:T(8,128)(2,1)} %param.36) | copy-start | bytes 36868
  11.7 7.1 %copy-start.13 = (bf16[2,2048,128]{2,1,0:T(8,128)(2,1)S(1)}, bf16[2,2048,128]{2,1,0:T(8,128)(2,1)}, u32[]{:S(2)}) copy-start(bf16[2,2048,128]{2,1,0:T(8,128)(2,1)} %param.23) | copy-start | bytes 3145732
  11.8 7.3 %copy-start.14 = (bf16[2,2048,128]{2,1,0:T(8,128)(2,1)S(1)}, bf16[2,2048,128]{2,1,0:T(8,128)(2,1)}, u32[]{:S(2)}) copy-start(bf16[2,2048,128]{2,1,0:T(8,128)(2,1)} %param.24) | copy-start | bytes 3145732
  14.6 9.5 %copy-start.6 = (bf16[2,4,512]{2,1,0:T(4,128)(2,1)S(1)}, bf16[2,4,512]{2,1,0:T(4,128)(2,1)}, u32[]{:S(2)}) copy-start(bf16[2,4,512]{2,1,0:T(4,128)(2,1)} %param.26) | copy-start | bytes 24580
  14.6 87.4 %copy-start.1 = (bf16[2,8,3,512]{3,1,2,0:T(8,128)(2,1)S(1)}, bf16[2,8,3,512]{3,1,2,0:T(8,128)(2,1)}, u32[]{:S(2)}) copy-start(bf16[2,8,3,512]{3,1,2,0:T(8,128)(2,1)} %param.34) | copy-start | bytes 147460
  14.6 93.8 %reduce-scatter.7.cloned.1.call-start = ((), (), s32[]{:S(2)}) async-start(), calls=%async_computation.5 | async-start | bytes 24576 | tf_op jit(solution)/shard_map/reduce_scatter | solution.py:45
  17.3 85.7 %copy-start.11 = (f32[2,8]{1,0:T(2,128)S(1)}, f32[2,8]{1,0:T(2,128)}, u32[]{:S(2)}) copy-start(f32[2,8]{1,0:T(2,128)} %param.30) | copy-start | bytes 196
  17.3 85.7 %copy-start.12 = (f32[2,8]{1,0:T(2,128)S(1)}, f32[2,8]{1,0:T(2,128)}, u32[]{:S(2)}) copy-start(f32[2,8]{1,0:T(2,128)} %param.29) | copy-start | bytes 196
  17.3 192.3 %all-gather.5.cloned.1.call-start = ((), (), s32[]{:S(2)}) async-start(), calls=%async_computation.8 | async-start | bytes 2228224 | tf_op jit(solution)/shard_map/all_gather | solution.py:108
  153.2 146.7 %reduce-scatter.9.cloned.1.call-start = ((), (), s32[]{:S(2)}) async-start(), calls=%async_computation.6 | async-start | bytes 24576 | tf_op jit(solution)/shard_map/reduce_scatter | solution.py:48
  224.4 80.8 %reduce-scatter.11.cloned.1.call-start = ((), (), s32[]{:S(2)}) async-start(), calls=%async_computation.7 | async-start | bytes 24576 | tf_op jit(solution)/shard_map/reduce_scatter | solution.py:45
  299.7 110.1 %all-gather.7.cloned.1.call-start = ((), (), s32[]{:S(2)}) async-start(), calls=%async_computation.9 | async-start | bytes 2228224 | tf_op jit(solution)/shard_map/all_gather | solution.py:108
  300.8 52.6 %copy-start.2 = (bf16[8,512]{1,0:T(8,128)(2,1)S(1)}, bf16[8,512]{1,0:T(8,128)(2,1)}, u32[]{:S(2)}) copy-start(bf16[8,512]{1,0:T(8,128)(2,1)} %reduce-scatter.5.cloned.1.call-done) | copy-start | bytes 24580
  300.8 53.8 %copy-start.3 = (bf16[8,512]{1,0:T(8,128)(2,1)S(1)}, bf16[8,512]{1,0:T(8,128)(2,1)}, u32[]{:S(2)}) copy-start(bf16[8,512]{1,0:T(8,128)(2,1)} %reduce-scatter.9.cloned.1.call-done) | copy-start | bytes 24580
Sparse Core Ops, SparseCore 0:
  14.7 10.0 reduce-scatter.4
  27.6 8.6 reduce-scatter.6
  153.3 56.2 all-gather.4
  224.6 6.2 reduce-scatter.8
  299.9 5.2 reduce-scatter.10
  353.5 56.2 all-gather.6
